TPU v7x, 32 devices: a whole 2x2x4 slice. The times are simulated.
32 devices in a mesh: fs: 8 (over z, y), tp: 4 (over x, core).
Axes of the slice: x: 2, y: 2, z: 4, core: 2. Of those that a mesh axis runs over, the one named last changes fastest.
Arguments:
- tokens: bfloat16 [640, 3072], P('tp'), may hold values from -6 to 6
- gain_first: float32 [3072], replicated, may hold values from 0.1 to 1.9
- gain_second: float32 [3072], replicated, may hold values from 0.1 to 1.9
- gate_first: float32 [3072, 8192], P('fs', 'tp'), may hold values from -0.109375 to 0.109375
- up_first: float32 [3072, 8192], P('fs', 'tp'), may hold values from -0.109375 to 0.109375
- down_first: float32 [8192, 3072], P('fs', 'tp'), may hold values from -0.09375 to 0.09375
- gate_second: float32 [3072, 8192], P('fs', 'tp'), may hold values from -0.109375 to 0.109375
- up_second: float32 [3072, 8192], P('fs', 'tp'), may hold values from -0.109375 to 0.109375
- down_second: float32 [8192, 3072], P('fs', 'tp'), may hold values from -0.09375 to 0.09375
Outputs:
- result_rows: bfloat16 [640, 3072], P('tp')
- serve_gate_first: bfloat16 [3072, 8192], P(None, 'fs')
- serve_up_first: bfloat16 [3072, 8192], P(None, 'fs')
- serve_down_first: bfloat16 [8192, 3072], P('fs')
- serve_gate_second: bfloat16 [3072, 8192], P(None, 'fs')
- serve_up_second: bfloat16 [3072, 8192], P(None, 'fs')
- serve_down_second: bfloat16 [8192, 3072], P('fs')
All inputs are finite; a program needn't handle non-finite values.
Results may differ from a plain program's by a relative error of at most 0.011.
Values may be sent and summed in bfloat16 or wider, within the bound.
A program may use at most 192 MiB of HBM per device.

v0:
```python
import jax
import jax.numpy as jnp
from jax import lax
from jax.sharding import PartitionSpec as P


def plain_norm(values):
    values = values.astype(jnp.float32)
    center = jnp.mean(values, axis=-1, keepdims=True)
    spread = jnp.mean(jnp.square(values - center), axis=-1, keepdims=True)
    return (values - center) * lax.rsqrt(spread + 1e-05)


def half_step(normed, scales, w_gate, w_rising, w_down):
    gate_part = jnp.dot(normed, w_gate, preferred_element_type=jnp.float32)
    rising = jnp.dot(normed, w_rising, preferred_element_type=jnp.float32)
    hidden = (jax.nn.silu(gate_part) * rising).astype(jnp.bfloat16)
    partial_value = jnp.dot(hidden, w_down, preferred_element_type=jnp.float32)
    block = lax.psum(partial_value, "fs")
    mixed = 1.6817928 * scales[None, :] * normed.astype(jnp.float32) + 0.5 * block
    return plain_norm(mixed).astype(jnp.bfloat16)


def on_device(
    tokens,
    gain_first,
    gain_second,
    gate_first,
    up_first,
    down_first,
    gate_second,
    up_second,
    down_second,
):
    row_count = gate_first.shape[0]
    offset = lax.axis_index("fs") * row_count

    def fold_gain(weight, scales):
        picked = lax.dynamic_slice_in_dim(scales, offset, row_count, 0)
        return (picked[:, None] * weight).astype(jnp.bfloat16)

    widened = (
        lax.all_gather(fold_gain(gate_first, gain_first), "tp", axis=1, tiled=True),
        lax.all_gather(fold_gain(up_first, gain_first), "tp", axis=1, tiled=True),
        lax.all_gather(fold_gain(gate_second, gain_second), "tp", axis=1, tiled=True),
        lax.all_gather(fold_gain(up_second, gain_second), "tp", axis=1, tiled=True),
        lax.all_gather(down_first.astype(jnp.bfloat16), "tp", axis=1, tiled=True),
        lax.all_gather(down_second.astype(jnp.bfloat16), "tp", axis=1, tiled=True),
    )
    regrouped = (
        lax.all_to_all(widened[0], "fs", split_axis=1, concat_axis=0, tiled=True),
        lax.all_to_all(widened[1], "fs", split_axis=1, concat_axis=0, tiled=True),
        lax.all_to_all(widened[2], "fs", split_axis=1, concat_axis=0, tiled=True),
        lax.all_to_all(widened[3], "fs", split_axis=1, concat_axis=0, tiled=True),
    )
    serve_gate_first, serve_up_first, serve_gate_second, serve_up_second = regrouped
    serve_down_first = widened[4]
    serve_down_second = widened[5]
    normed_zero = plain_norm(tokens).astype(jnp.bfloat16)
    normed_one = half_step(
        normed_zero, gain_first, serve_gate_first, serve_up_first, serve_down_first
    )
    result_rows = half_step(
        normed_one, gain_second, serve_gate_second, serve_up_second, serve_down_second
    )
    return (
        result_rows,
        serve_gate_first,
        serve_up_first,
        serve_down_first,
        serve_gate_second,
        serve_up_second,
        serve_down_second,
    )


def solution(mesh):
    placed = (
        P("tp", None),
        P(),
        P(),
        P("fs", "tp"),
        P("fs", "tp"),
        P("fs", "tp"),
        P("fs", "tp"),
        P("fs", "tp"),
        P("fs", "tp"),
    )
    return jax.shard_map(
        on_device,
        mesh=mesh,
        in_specs=placed,
        out_specs=(
            P("tp", None),
            P(None, "fs"),
            P(None, "fs"),
            P("fs", None),
            P(None, "fs"),
            P(None, "fs"),
            P("fs", None),
        ),
        check_vma=False,
    )
```

profile of v0, /device:TPU:0, one launch (start us, length us, event | category | flops | bytes accessed | tf_op | source)
XLA Modules:
  0.0 865.7 jit_solution(17595812001735718184)
XLA Ops:
  8.0 5.5 multiply_convert_fusion.3
  14.3 48.5 %all-gather.7.cloned.1.call-done = bf16[384,8192]{1,0:T(8,128)(2,1)} async-done(((bf16[384,2048]{1,0:T(8,128)(2,1)}), bf16[384,8192]{1,0:T(8,128)(2,1)}) %all-gather.7.cloned.1.call-update) | async-done | bytes 6291472 | tf_op jit(solution)/shard_map/all_gather | solution.py:43
  62.7 6.5 copy.31
  69.2 5.8 all-to-all-start
  75.2 4.7 multiply_convert_fusion.1
  79.9 31.4 %all-gather.9.cloned.1.call-done = bf16[384,8192]{1,0:T(8,128)(2,1)} async-done(((bf16[384,2048]{1,0:T(8,128)(2,1)}), bf16[384,8192]{1,0:T(8,128)(2,1)}) %all-gather.9.cloned.1.call-update) | async-done | bytes 6291472 | tf_op jit(solution)/shard_map/all_gather | solution.py:44
  111.3 6.5 copy.30
  117.8 95.9 %all-to-all-done = bf16[384,8,1024]{2,0,1:T(8,128)(2,1)} async-done(((bf16[384,8,1024]{2,0,1:T(8,128)(2,1)}), bf16[384,8,1024]{2,0,1:T(8,128)(2,1)}, u32[]{:S(2)}, u32[]{:S(2)}) %all-to-all-start) | async-done | bytes 6291488 | tf_op jit(solution)/shard_map/all_to_all | solution.py:51
  213.7 5.0 all-to-all-start.1
  220.1 6.5 copy.29
  226.6 129.8 %all-to-all-done.1 = bf16[384,8,1024]{2,0,1:T(8,128)(2,1)} async-done(((bf16[384,8,1024]{2,0,1:T(8,128)(2,1)}), bf16[384,8,1024]{2,0,1:T(8,128)(2,1)}, u32[]{:S(2)}, u32[]{:S(2)}) %all-to-all-start.1) | async-done | bytes 6291488 | tf_op jit(solution)/shard_map/all_to_all | solution.py:52
  356.4 4.8 all-to-all-start.2
  363.0 4.0 fusion.16
  367.1 8.9 %fusion.7 = f32[160,3072]{1,0:T(8,128)} fusion(bf16[1024,3072]{1,0:T(8,128)(2,1)} %all-gather.11.cloned.1.call-done, bf16[3072,1024]{1,0:T(8,128)(2,1)} %bitcast.3, f32[160,1024]{1,0:T(8,128)S(1)} %fusion.16, bf16[160,3072]{1,0:T(8,128)(2,1)S(1)} %copy-done, f32[160]{0:T(256)S(1)} %add_rsqrt_fusion.2, f32[160]{0:T(256)S(1)} %broadcast_multiply_fusion.4), kind=kOutput, calls=%fused_computation.25 | convolution fusion | flops 2016215040 | bytes 16188672 | tf_op jit(solution)/shard_map/dot_general | solution.py:18
  376.0 34.6 %all-gather.15.cloned.1.call-done = bf16[384,8192]{1,0:T(8,128)(2,1)} async-done(((bf16[384,2048]{1,0:T(8,128)(2,1)}), bf16[384,8192]{1,0:T(8,128)(2,1)}) %all-gather.15.cloned.1.call-update) | async-done | bytes 6291472 | tf_op jit(solution)/shard_map/all_gather | solution.py:46
  410.6 6.5 copy.28
  417.1 107.7 %all-to-all-done.2 = bf16[384,8,1024]{2,0,1:T(8,128)(2,1)} async-done(((bf16[384,8,1024]{2,0,1:T(8,128)(2,1)}), bf16[384,8,1024]{2,0,1:T(8,128)(2,1)}, u32[]{:S(2)}, u32[]{:S(2)}) %all-to-all-start.2) | async-done | bytes 6291488 | tf_op jit(solution)/shard_map/all_to_all | solution.py:53
  524.8 4.8 all-to-all-start.3
  529.7 3.3 convert_element_type.54
  533.2 138.3 %all-reduce.3.cloned.1.call-done = f32[160,3072]{1,0:T(8,128)} async-done(((f32[160,3072]{1,0:T(8,128)}), f32[160,3072]{1,0:T(8,128)}) %all-reduce.3.cloned.1.call-update) | async-done | bytes 1966096 | tf_op jit(solution)/shard_map/psum | solution.py:19
  671.5 2.3 fusion.10
  675.5 4.7 fusion.18
  680.1 36.9 %all-gather.17.cloned.1.call-done = bf16[1024,3072]{1,0:T(8,128)(2,1)} async-done(((bf16[1024,768]{1,0:T(8,128)(2,1)}), bf16[1024,3072]{1,0:T(8,128)(2,1)}) %all-gather.17.cloned.1.call-update) | async-done | bytes 6291472 | tf_op jit(solution)/shard_map/all_gather | solution.py:48
  717.1 8.2 fusion.6
  725.3 98.6 %all-reduce.5.cloned.1.call-done = f32[160,3072]{1,0:T(8,128)} async-done(((f32[160,3072]{1,0:T(8,128)}), f32[160,3072]{1,0:T(8,128)}) %all-reduce.5.cloned.1.call-update) | async-done | bytes 1966096 | tf_op jit(solution)/shard_map/psum | solution.py:19
  823.8 2.1 fusion.11
  828.0 6.4 copy.40
  834.4 6.3 copy.41
  840.7 2.7 copy.42
  843.4 6.4 copy.43
  849.8 6.3 copy.44
  856.2 2.7 copy.45
  (60 shorter events, 9.0 us)
Async XLA Ops:
  7.2 55.6 %all-gather.7.cloned.1.call-start = ((), (), s32[]{:S(2)}) async-start(), calls=%async_computation.4 | async-start | bytes 7864320 | tf_op jit(solution)/shard_map/all_gather | solution.py:43
  13.5 97.7 %all-gather.9.cloned.1.call-start = ((), (), s32[]{:S(2)}) async-start(), calls=%async_computation.5 | async-start | bytes 7864320 | tf_op jit(solution)/shard_map/all_gather | solution.py:44
  69.2 5.8 copy-start.6
  69.2 5.9 copy-start.3
  69.2 144.4 %all-to-all-start = ((bf16[384,8,1024]{2,0,1:T(8,128)(2,1)}), bf16[384,8,1024]{2,0,1:T(8,128)(2,1)}, u32[]{:S(2)}, u32[]{:S(2)}) async-start(bf16[384,8,1024]{2,0,1:T(8,128)(2,1)} %bitcast.38), calls=%async_computation | async-start | bytes 12582912 | tf_op jit(solution)/shard_map/all_to_all | solution.py:51
  75.0 145.1 %all-gather.13.cloned.1.call-start = ((), (), s32[]{:S(2)}) async-start(), calls=%async_computation.8 | async-start | bytes 7864320 | tf_op jit(solution)/shard_map/all_gather | solution.py:45
  213.7 5.1 copy-start.4
  213.7 142.7 %all-to-all-start.1 = ((bf16[384,8,1024]{2,0,1:T(8,128)(2,1)}), bf16[384,8,1024]{2,0,1:T(8,128)(2,1)}, u32[]{:S(2)}, u32[]{:S(2)}) async-start(bf16[384,8,1024]{2,0,1:T(8,128)(2,1)} %bitcast.39), calls=%async_computation.1 | async-start | bytes 12582912 | tf_op jit(solution)/shard_map/all_to_all | solution.py:52
  218.7 148.4 %all-gather.11.cloned.1.call-start = ((), (), s32[]{:S(2)}) async-start(), calls=%async_computation.6 | async-start | bytes 7864320 | tf_op jit(solution)/shard_map/all_gather | solution.py:47
  356.4 168.4 %all-to-all-start.2 = ((bf16[384,8,1024]{2,0,1:T(8,128)(2,1)}), bf16[384,8,1024]{2,0,1:T(8,128)(2,1)}, u32[]{:S(2)}, u32[]{:S(2)}) async-start(bf16[384,8,1024]{2,0,1:T(8,128)(2,1)} %bitcast.36), calls=%async_computation.2 | async-start | bytes 12582912 | tf_op jit(solution)/shard_map/all_to_all | solution.py:53
  361.2 1.2 copy-start
  361.2 49.4 %all-gather.15.cloned.1.call-start = ((), (), s32[]{:S(2)}) async-start(), calls=%async_computation.9 | async-start | bytes 7864320 | tf_op jit(solution)/shard_map/all_gather | solution.py:46
  361.8 309.7 %all-reduce.3.cloned.1.call-start = ((), (), s32[]{:S(2)}) async-start(), calls=%async_computation.7 | async-start | bytes 3932160 | tf_op jit(solution)/shard_map/psum | solution.py:19
  524.8 192.3 %all-to-all-start.3 = ((bf16[384,8,1024]{2,0,1:T(8,128)(2,1)}), bf16[384,8,1024]{2,0,1:T(8,128)(2,1)}, u32[]{:S(2)}, u32[]{:S(2)}) async-start(bf16[384,8,1024]{2,0,1:T(8,128)(2,1)} %bitcast.37), calls=%async_computation.3 | async-start | bytes 12582912 | tf_op jit(solution)/shard_map/all_to_all | solution.py:54
  529.6 3.6 copy-start.5
  529.6 187.4 %all-gather.17.cloned.1.call-start = ((), (), s32[]{:S(2)}) async-start(), calls=%async_computation.10 | async-start | bytes 7864320 | tf_op jit(solution)/shard_map/all_gather | solution.py:48
  533.0 290.8 %all-reduce.5.cloned.1.call-start = ((), (), s32[]{:S(2)}) async-start(), calls=%async_computation.11 | async-start | bytes 3932160 | tf_op jit(solution)/shard_map/psum | solution.py:19
  671.5 2.3 copy-start.1
  823.8 2.1 copy-start.2
  828.0 12.7 %slice-start = ((s8[6291456]{0:T(1024)(128)(4,1)}), s8[4194304]{0:T(1024)(128)(4,1)S(1)}, s32[]{:S(2)}) async-start(s8[6291456]{0:T(1024)(128)(4,1)} %bitcast.40), calls=%async_computation.12 | async-start | bytes 8388608
  834.4 6.4 slice-start.1
  843.4 12.7 %slice-start.2 = ((s8[6291456]{0:T(1024)(128)(4,1)}), s8[4194304]{0:T(1024)(128)(4,1)S(1)}, s32[]{:S(2)}) async-start(s8[6291456]{0:T(1024)(128)(4,1)} %bitcast.42), calls=%async_computation.14 | async-start | bytes 8388608
  849.8 6.4 slice-start.3
Sparse Core Ops, SparseCore 0:
  13.6 49.0 all-gather.6
  64.9 46.3 all-gather.8
  113.4 46.3 all-gather.12
  221.3 46.7 all-gather.10
  363.8 46.7 all-gather.14
  414.6 256.8 all-reduce.2
  673.6 43.3 all-gather.16
  725.4 98.3 all-reduce.4
where the time goes:
time: 866 us
  waiting for transfers between devices  723 us (83%)
  local copies, waits for them, and re-layouts  58.3 us (7%)
  matrix products  25.7 us (3%)
  other arithmetic  23.5 us (3%)
  starting transfers between devices  20.9 us (2%)
  between operations  14.3 us (2%)
    psum x2, waiting for transfers between devices, half_step(): block = lax.psum(partial_value, 'fs')  237 us
    all_to_all x1, waiting for transfers between devices, on_device(): lax.all_to_all(widened[1], 'fs', split_axis=1, concat_axis=0, tiled=True)  130 us
    all_to_all x1, waiting for transfers between devices, on_device(): lax.all_to_all(widened[2], 'fs', split_axis=1, concat_axis=0, tiled=True)  108 us
    all_to_all x1, waiting for transfers between devices, on_device(): lax.all_to_all(widened[0], 'fs', split_axis=1, concat_axis=0, tiled=True)  95.9 us
    all_gather x1, waiting for transfers between devices, on_device(): lax.all_gather(fold_gain(gate_first, gain_first), 'tp', axis=1, tiled=True)  48.5 us
    all_gather x1, waiting for transfers between devices, on_device(): lax.all_gather(down_second.astype(jnp.bfloat16), 'tp', axis=1, tiled=True)  36.9 us
    all_gather x1, waiting for transfers between devices, on_device(): lax.all_gather(fold_gain(up_second, gain_second), 'tp', axis=1, tiled=True)  34.6 us
    unnamed x28, local copies, waits for them, and re-layouts  31.5 us
  transfers between devices with their start and end apart: 12, of which 9 were waited for; matrix products, arithmetic and copies ran while one was open for 7% of the time, Pallas kernels for 0%

commit v1 on v0

--- a/solution.py
+++ b/solution.py
@@ -16,7 +16,7 @@
     rising = jnp.dot(normed, w_rising, preferred_element_type=jnp.float32)
     hidden = (jax.nn.silu(gate_part) * rising).astype(jnp.bfloat16)
     partial_value = jnp.dot(hidden, w_down, preferred_element_type=jnp.float32)
-    block = lax.psum(partial_value, "fs")
+    block = jnp.sum(lax.all_gather(partial_value, "fs"), axis=0)
     mixed = 1.6817928 * scales[None, :] * normed.astype(jnp.float32) + 0.5 * block
     return plain_norm(mixed).astype(jnp.bfloat16)
 

time: 866 us -> 1110 us (1.28)
  waiting for transfers between devices: 723 us -> 957 us
    all_gather x0 -> x2, waiting for transfers between devices: none -> 340 us  [half_step(): block = jnp.sum(lax.all_gather(partial_value, 'fs'), axis=0)]
    psum x2 -> x0, waiting for transfers between devices: 237 us -> none  [half_step(): block = lax.psum(partial_value, 'fs')]
    all_to_all x1, waiting for transfers between devices: 108 us -> 279 us  [on_device(): lax.all_to_all(widened[2], 'fs', split_axis=1, concat_axis=0, tiled=True)]
    all_gather x1, waiting for transfers between devices: 34.6 us -> 0.02 us  [on_device(): lax.all_gather(fold_gain(up_second, gain_second), 'tp', axis=1, tiled=True)]
    reduce_sum x0 -> x2, other arithmetic: none -> 14.5 us  [half_step(): block = jnp.sum(lax.all_gather(partial_value, 'fs'), axis=0)]
  transfers between devices with their start and end apart: 12 -> 12, of which waited for: 9 -> 8; matrix products, arithmetic and copies ran while one was open for 7% -> 6% of each run, Pallas kernels for 0% -> 0%
where the time goes in v1:
time: 1110 us
  waiting for transfers between devices  957 us (86%)
  local copies, waits for them, and re-layouts  60.7 us (5%)
  other arithmetic  34.4 us (3%)
  matrix products  24.8 us (2%)
  starting transfers between devices  20.8 us (2%)
  between operations  14.3 us (1%)
    all_gather x2, waiting for transfers between devices, half_step(): block = jnp.sum(lax.all_gather(partial_value, 'fs'), axis=0)  340 us
    all_to_all x1, waiting for transfers between devices, on_device(): lax.all_to_all(widened[2], 'fs', split_axis=1, concat_axis=0, tiled=True)  279 us
    all_to_all x1, waiting for transfers between devices, on_device(): lax.all_to_all(widened[1], 'fs', split_axis=1, concat_axis=0, tiled=True)  132 us
    all_to_all x1, waiting for transfers between devices, on_device(): lax.all_to_all(widened[0], 'fs', split_axis=1, concat_axis=0, tiled=True)  95.9 us
    all_gather x1, waiting for transfers between devices, on_device(): lax.all_gather(fold_gain(gate_first, gain_first), 'tp', axis=1, tiled=True)  46 us
    unnamed x28, local copies, waits for them, and re-layouts  33.4 us
    all_gather x1, waiting for transfers between devices, on_device(): lax.all_gather(down_second.astype(jnp.bfloat16), 'tp', axis=1, tiled=True)  31.6 us
    all_gather x1, waiting for transfers between devices, on_device(): lax.all_gather(fold_gain(up_first, gain_first), 'tp', axis=1, tiled=True)  31.4 us
  transfers between devices with their start and end apart: 12, of which 8 were waited for; matrix products, arithmetic and copies ran while one was open for 6% of the time, Pallas kernels for 0%

profile of v1, /device:TPU:0, one launch (start us, length us, event | category | flops | bytes accessed | tf_op | source)
XLA Modules:
  0.0 1111.8 jit_solution(16521788933453034060)
XLA Ops:
  8.0 5.5 multiply_convert_fusion.3
  16.7 46.0 %all-gather.11.cloned.1.call-done = bf16[384,8192]{1,0:T(8,128)(2,1)} async-done(((bf16[384,2048]{1,0:T(8,128)(2,1)}), bf16[384,8192]{1,0:T(8,128)(2,1)}) %all-gather.11.cloned.1.call-update) | async-done | bytes 6291472 | tf_op jit(solution)/shard_map/all_gather | solution.py:43
  62.7 6.5 copy.31
  69.2 5.8 all-to-all-start
  75.2 4.7 multiply_convert_fusion.1
  79.9 31.4 %all-gather.13.cloned.1.call-done = bf16[384,8192]{1,0:T(8,128)(2,1)} async-done(((bf16[384,2048]{1,0:T(8,128)(2,1)}), bf16[384,8192]{1,0:T(8,128)(2,1)}) %all-gather.13.cloned.1.call-update) | async-done | bytes 6291472 | tf_op jit(solution)/shard_map/all_gather | solution.py:44
  111.3 6.5 copy.30
  117.8 95.9 %all-to-all-done = bf16[384,8,1024]{2,0,1:T(8,128)(2,1)} async-done(((bf16[384,8,1024]{2,0,1:T(8,128)(2,1)}), bf16[384,8,1024]{2,0,1:T(8,128)(2,1)}, u32[]{:S(2)}, u32[]{:S(2)}) %all-to-all-start) | async-done | bytes 6291488 | tf_op jit(solution)/shard_map/all_to_all | solution.py:51
  213.7 4.8 all-to-all-start.1
  220.3 4.0 fusion.16
  224.3 131.8 %all-to-all-done.1 = bf16[384,8,1024]{2,0,1:T(8,128)(2,1)} async-done(((bf16[384,8,1024]{2,0,1:T(8,128)(2,1)}), bf16[384,8,1024]{2,0,1:T(8,128)(2,1)}, u32[]{:S(2)}, u32[]{:S(2)}) %all-to-all-start.1) | async-done | bytes 6291488 | tf_op jit(solution)/shard_map/all_to_all | solution.py:52
  356.1 8.2 fusion.7
  364.4 6.9 copy.29
  371.3 5.0 all-to-all-start.2
  376.3 6.5 copy.28
  382.8 278.8 %all-to-all-done.2 = bf16[384,8,1024]{2,0,1:T(8,128)(2,1)} async-done(((bf16[384,8,1024]{2,0,1:T(8,128)(2,1)}), bf16[384,8,1024]{2,0,1:T(8,128)(2,1)}, u32[]{:S(2)}, u32[]{:S(2)}) %all-to-all-start.2) | async-done | bytes 6291488 | tf_op jit(solution)/shard_map/all_to_all | solution.py:53
  661.6 4.8 all-to-all-start.3
  666.4 3.2 convert_element_type.54
  669.9 125.4 %all-gather.23.cloned.1.call-done = f32[1280,3072]{1,0:T(8,128)} async-done(((f32[160,3072]{1,0:T(8,128)}), f32[1280,3072]{1,0:T(8,128)}) %all-gather.23.cloned.1.call-update) | async-done | bytes 15728656 | tf_op jit(solution)/shard_map/all_gather | solution.py:19
  795.3 7.2 reduce_sum.74
  805.7 4.1 fusion.18
  809.8 31.6 %all-gather.21.cloned.1.call-done = bf16[1024,3072]{1,0:T(8,128)(2,1)} async-done(((bf16[1024,768]{1,0:T(8,128)(2,1)}), bf16[1024,3072]{1,0:T(8,128)(2,1)}) %all-gather.21.cloned.1.call-update) | async-done | bytes 6291472 | tf_op jit(solution)/shard_map/all_gather | solution.py:48
  841.4 8.4 fusion.6
  849.9 214.6 %all-gather.25.cloned.1.call-done = f32[1280,3072]{1,0:T(8,128)} async-done(((f32[160,3072]{1,0:T(8,128)}), f32[1280,3072]{1,0:T(8,128)}) %all-gather.25.cloned.1.call-update) | async-done | bytes 15728656 | tf_op jit(solution)/shard_map/all_gather | solution.py:19
  1064.5 7.3 reduce_sum.77
  1072.7 1.4 multiply_convert_fusion.4
  1074.1 6.4 copy.38
  1080.5 6.3 copy.39
  1086.9 2.7 copy.40
  1089.6 6.4 copy.41
  1095.9 6.3 copy.42
  1102.3 2.7 copy.43
  (62 shorter events, 10.5 us)
Async XLA Ops:
  7.2 55.6 %all-gather.11.cloned.1.call-start = ((), (), s32[]{:S(2)}) async-start(), calls=%async_computation.4 | async-start | bytes 7864320 | tf_op jit(solution)/shard_map/all_gather | solution.py:43
  13.5 1.9 copy-start.4
  13.5 97.7 %all-gather.13.cloned.1.call-start = ((), (), s32[]{:S(2)}) async-start(), calls=%async_computation.5 | async-start | bytes 7864320 | tf_op jit(solution)/shard_map/all_gather | solution.py:44
  14.3 210.1 %all-gather.15.cloned.1.call-start = ((), (), s32[]{:S(2)}) async-start(), calls=%async_computation.6 | async-start | bytes 7864320 | tf_op jit(solution)/shard_map/all_gather | solution.py:47
  69.2 5.8 copy-start.6
  69.2 5.9 copy-start.3
  69.2 144.4 %all-to-all-start = ((bf16[384,8,1024]{2,0,1:T(8,128)(2,1)}), bf16[384,8,1024]{2,0,1:T(8,128)(2,1)}, u32[]{:S(2)}, u32[]{:S(2)}) async-start(bf16[384,8,1024]{2,0,1:T(8,128)(2,1)} %bitcast.40), calls=%async_computation | async-start | bytes 12582912 | tf_op jit(solution)/shard_map/all_to_all | solution.py:51
  75.0 289.4 %all-gather.17.cloned.1.call-start = ((), (), s32[]{:S(2)}) async-start(), calls=%async_computation.7 | async-start | bytes 7864320 | tf_op jit(solution)/shard_map/all_gather | solution.py:45
  213.7 142.5 %all-to-all-start.1 = ((bf16[384,8,1024]{2,0,1:T(8,128)(2,1)}), bf16[384,8,1024]{2,0,1:T(8,128)(2,1)}, u32[]{:S(2)}, u32[]{:S(2)}) async-start(bf16[384,8,1024]{2,0,1:T(8,128)(2,1)} %bitcast.39), calls=%async_computation.1 | async-start | bytes 12582912 | tf_op jit(solution)/shard_map/all_to_all | solution.py:52
  218.4 1.2 copy-start
  218.4 157.8 %all-gather.19.cloned.1.call-start = ((), (), s32[]{:S(2)}) async-start(), calls=%async_computation.8 | async-start | bytes 7864320 | tf_op jit(solution)/shard_map/all_gather | solution.py:46
  219.0 576.2 %all-gather.23.cloned.1.call-start = ((), (), s32[]{:S(2)}) async-start(), calls=%async_computation.10 | async-start | bytes 17694720 | tf_op jit(solution)/shard_map/all_gather | solution.py:19
  371.3 290.3 %all-to-all-start.2 = ((bf16[384,8,1024]{2,0,1:T(8,128)(2,1)}), bf16[384,8,1024]{2,0,1:T(8,128)(2,1)}, u32[]{:S(2)}, u32[]{:S(2)}) async-start(bf16[384,8,1024]{2,0,1:T(8,128)(2,1)} %bitcast.41), calls=%async_computation.2 | async-start | bytes 12582912 | tf_op jit(solution)/shard_map/all_to_all | solution.py:53
  661.6 179.8 %all-to-all-start.3 = ((bf16[384,8,1024]{2,0,1:T(8,128)(2,1)}), bf16[384,8,1024]{2,0,1:T(8,128)(2,1)}, u32[]{:S(2)}, u32[]{:S(2)}) async-start(bf16[384,8,1024]{2,0,1:T(8,128)(2,1)} %bitcast.38), calls=%async_computation.3 | async-start | bytes 12582912 | tf_op jit(solution)/shard_map/all_to_all | solution.py:54
  666.4 3.5 copy-start.5
  666.4 175.0 %all-gather.21.cloned.1.call-start = ((), (), s32[]{:S(2)}) async-start(), calls=%async_computation.9 | async-start | bytes 7864320 | tf_op jit(solution)/shard_map/all_gather | solution.py:48
  669.6 394.8 %all-gather.25.cloned.1.call-start = ((), (), s32[]{:S(2)}) async-start(), calls=%async_computation.11 | async-start | bytes 17694720 | tf_op jit(solution)/shard_map/all_gather | solution.py:19
  804.7 0.9 copy-start.1
  1064.5 7.3 copy-start.2
  1074.1 12.7 %slice-start = ((s8[6291456]{0:T(1024)(128)(4,1)}), s8[4194304]{0:T(1024)(128)(4,1)S(1)}, s32[]{:S(2)}) async-start(s8[6291456]{0:T(1024)(128)(4,1)} %bitcast.44), calls=%async_computation.12 | async-start | bytes 8388608
  1080.5 6.4 slice-start.1
  1089.6 12.7 %slice-start.2 = ((s8[6291456]{0:T(1024)(128)(4,1)}), s8[4194304]{0:T(1024)(128)(4,1)S(1)}, s32[]{:S(2)}) async-start(s8[6291456]{0:T(1024)(128)(4,1)} %bitcast.46), calls=%async_computation.14 | async-start | bytes 8388608
  1095.9 6.4 slice-start.3
Sparse Core Ops, SparseCore 0:
  13.6 49.0 all-gather.10
  64.9 46.3 all-gather.12
  113.4 46.3 all-gather.14
  161.8 46.3 all-gather.16
  221.1 46.7 all-gather.18
  364.5 430.7 all-gather.22
  797.4 43.9 all-gather.20
  850.0 214.4 all-gather.24
